TPU v7x, 32 devices: a whole 2x2x4 slice. The times are simulated.
32 devices in a mesh: ep: 8 (over z, x), tp: 4 (over y, core).
Axes of the slice: x: 2, y: 2, z: 4, core: 2. Of those that a mesh axis runs over, the one named last changes fastest.
Arguments:
- tokens: bfloat16 [1024, 2048], P('ep'), may hold values from -6 to 6
- norm_gain: float32 [2048], replicated, may hold values from 0.1 to 1.9
- expert_ids: int32 [1024, 2], P('ep'), may hold values from 0 to 7, all different within a row; in each aligned block of 128 rows (0 to 127, 128 to 255, ...) at most 64 rows name the same one
- route_weights: float32 [1024, 2], P('ep'), may hold values from 0.2 to 1
- w_gate: bfloat16 [8, 2048, 4096], P('ep', None, 'tp'), may hold values from -0.125 to 0.125
- w_up: bfloat16 [8, 2048, 4096], P('ep', None, 'tp'), may hold values from -0.125 to 0.125
- w_down: bfloat16 [8, 4096, 2048], P('ep', 'tp'), may hold values from -0.09375 to 0.09375
Outputs:
- combined: bfloat16 [1024, 2048], P('ep', 'tp')
Inputs may be any that keep to these rules, and one draw needn't show every extreme that they name: `expert_ids`: each row names two different experts; among the rows of one device no expert is named more than 64 times, and in every draw some expert is named exactly 64 times there.
All inputs are finite; a program needn't handle non-finite values.
Results may differ from a plain program's by a relative error of at most 0.019.
Values may be sent and summed in bfloat16 or wider, within the bound.
A program may use at most 64 MiB of HBM per device.

v0:
```python
import jax
import jax.numpy as jnp
from jax import lax
from jax.sharding import PartitionSpec as P

epsilon = 1e-06


def per_device(tokens, norm_gain, expert_ids, route_weights, w_gate, w_up, w_down):
    tok_rows, model_width = tokens.shape
    local_count = w_gate.shape[0]
    experts = local_count * lax.axis_size("ep")
    rank_count = lax.axis_size("tp")
    column_width = model_width // rank_count
    capacity = 4 * tok_rows // experts
    as_float = tokens.astype(jnp.float32)
    scale = lax.rsqrt(jnp.mean(as_float * as_float, axis=-1, keepdims=True) + epsilon)
    normed = (as_float * scale * norm_gain[None, :]).astype(jnp.bfloat16)
    flat_ids = expert_ids.reshape(-1)
    one_hot = (flat_ids[:, None] == jnp.arange(experts, dtype=jnp.int32)[None, :]).astype(jnp.int32)
    slot_index = jnp.sum((jnp.cumsum(one_hot, axis=0) - one_hot) * one_hot, axis=1)
    target = flat_ids * capacity + slot_index
    token_rows = jnp.repeat(normed, 2, axis=0)
    token_rows = lax.dynamic_slice_in_dim(
        token_rows, lax.axis_index("tp") * column_width, column_width, 1
    )
    outgoing = (
        jnp.zeros((experts * capacity, token_rows.shape[1]), jnp.bfloat16)
        .at[target]
        .set(token_rows)
    )
    outgoing = outgoing.reshape(experts, capacity, token_rows.shape[1])
    arrived = lax.all_to_all(outgoing, "ep", split_axis=0, concat_axis=1, tiled=True)
    piece = lax.all_gather(arrived, "tp", axis=2, tiled=True)
    gate_part = jnp.einsum("erd,edf->erf", piece, w_gate, preferred_element_type=jnp.float32)
    up_part = jnp.einsum("erd,edf->erf", piece, w_up, preferred_element_type=jnp.float32)
    hidden = (jax.nn.silu(gate_part) * up_part).astype(jnp.bfloat16)
    partial_value = jnp.einsum("erf,efd->erd", hidden, w_down, preferred_element_type=jnp.float32)
    summed = lax.psum_scatter(
        partial_value.astype(jnp.bfloat16), "tp", scatter_dimension=2, tiled=True
    )
    returned = lax.all_to_all(summed, "ep", split_axis=1, concat_axis=0, tiled=True)
    picked = returned.reshape(experts * capacity, column_width)[target]
    picked = picked.reshape(tok_rows, 2, column_width).astype(jnp.float32)
    return jnp.sum(picked * route_weights[:, :, None], axis=1).astype(jnp.bfloat16)


def solution(mesh):
    in_specs = (
        P("ep", None),
        P(),
        P("ep", None),
        P("ep", None),
        P("ep", None, "tp"),
        P("ep", None, "tp"),
        P("ep", "tp", None),
    )
    out_specs = P("ep", "tp")
    return jax.shard_map(
        per_device, mesh=mesh, in_specs=in_specs, out_specs=out_specs, check_vma=False
    )
```

profile of v0, /device:TPU:0, one launch (start us, length us, event | category | flops | bytes accessed | tf_op | source)
XLA Modules:
  0.0 143.9 jit_solution(12117852993632384072)
XLA Ops:
  6.5 0.8 copy.19
  7.6 0.7 broadcast_multiply_fusion
  8.3 0.6 reduce-window.6
  9.4 1.2 fusion.18
  10.6 1.2 fusion.20
  11.9 0.6 broadcast_in_dim.5
  12.5 0.4 reshape.102
  13.0 1.7 %scatter_custom_fusion = bf16[512,512]{1,0:T(8,128)(2,1)S(1)} fusion(s32[256]{0:T(256)S(1)} %bitcast.52, bf16[256,2048]{1,0:T(8,128)(2,1)S(1)} %reshape.102, s32[]{:T(128)} %constant.12.clone.1, s32[]{:T(128)S(6)} %select_n.15, bf16[]{:T(256)} %constant.10.clone.1), kind=kCustom, calls=%fused_computation.20 | custom fusion | bytes 786442 | tf_op jit(solution)/shard_map/scatter | solution.py:30
  14.7 21.7 %all_to_all.21 = bf16[8,64,512]{2,1,0:T(8,128)(2,1)} all-to-all(bf16[8,64,512]{2,1,0:T(8,128)(2,1)S(1)} %bitcast.51), channel_id=1, replica_groups=mesh['ep'=8,'tp'=4] {'ep'}, dimensions={0} | all-to-all | bytes 1048576 | tf_op jit(solution)/shard_map/all_to_all | solution.py:33
  36.5 0.2 reduce-scatter.2.cloned.1.call-start
  36.7 21.5 %all-gather.2.cloned.1.call-done = bf16[1,512,2048]{2,1,0:T(8,128)(2,1)} async-done(((bf16[1,512,512]{2,1,0:T(8,128)(2,1)}), bf16[1,512,2048]{2,1,0:T(8,128)(2,1)}) %all-gather.2.cloned.1.call-update) | async-done | bytes 2097168 | tf_op jit(solution)/shard_map/all_gather | solution.py:34
  58.2 6.6 %fusion.4 = f32[512,1024]{1,0:T(8,128)} fusion(bf16[1,2048,1024]{2,1,0:T(8,128)(2,1)} %param.11, bf16[1,512,2048]{2,1,0:T(8,128)(2,1)} %all-gather.2.cloned.1.call-done), kind=kOutput, calls=%fused_computation.6 | convolution fusion | flops 2147483648 | bytes 8388608 | tf_op jit(solution)/shard_map/erd,edf->erf/dot_general | solution.py:35
  64.8 10.0 %fusion.9 = bf16[1,512,2048]{2,1,0:T(8,128)(2,1)} fusion(bf16[1,1024,2048]{2,1,0:T(8,128)(2,1)} %param.13, f32[512,1024]{1,0:T(8,128)} %fusion.4, bf16[1,2048,1024]{2,1,0:T(8,128)(2,1)} %param.12, bf16[1,512,2048]{2,1,0:T(8,128)(2,1)S(1)} %copy-done.1), kind=kOutput, calls=%fused_computation.9 | convolution fusion | flops 4299161600 | bytes 14680064 | tf_op jit(solution)/shard_map/erf,efd->erd/dot_general | solution.py:38
  74.8 31.3 %reduce-scatter.2.cloned.1.call-done = bf16[1,512,512]{2,1,0:T(8,128)(2,1)} async-done(((bf16[1,512,2048]{2,1,0:T(8,128)(2,1)}), bf16[1,512,512]{2,1,0:T(8,128)(2,1)}) %reduce-scatter.2.cloned.1.call-update) | async-done | bytes 524304 | tf_op jit(solution)/shard_map/reduce_scatter | solution.py:39
  106.2 1.9 %copy.27 = bf16[1,512,512]{2,0,1:T(2,128)(2,1)S(1)} copy(bf16[1,512,512]{2,1,0:T(8,128)(2,1)} %reduce-scatter.2.cloned.1.call-done) | data formatting | bytes 1048576 | tf_op jit(solution)/shard_map/reduce_scatter | solution.py:39
  108.0 0.5 broadcast.73
  108.5 4.0 %reduce.2 = bf16[512,512]{1,0:T(8,128)(2,1)S(1)} reduce(bf16[512,1,512]{2,1,0:T(2,128)(2,1)S(1)} %bitcast.49, bf16[]{:T(256)} %broadcast.73), dimensions={1}, to_apply=%bitcast.46.reduce_sub_computation | reduce | bytes 1048578
  112.5 1.2 reshape.129
  113.7 5.5 %all-to-all-start.1 = ((bf16[8,2,16384]{2,1,0:T(2,128)(2,1)}), bf16[8,2,16384]{2,1,0:T(2,128)(2,1)S(1)}, u32[]{:S(2)}, u32[]{:S(2)}) async-start(bf16[8,2,16384]{2,1,0:T(2,128)(2,1)} %reshape.129), calls=%async_computation.2 | async-start | bytes 1048576 | tf_op jit(solution)/shard_map/all_to_all | solution.py:42
  119.3 14.2 %all-to-all-done.1 = bf16[8,2,16384]{2,1,0:T(2,128)(2,1)S(1)} async-done(((bf16[8,2,16384]{2,1,0:T(2,128)(2,1)}), bf16[8,2,16384]{2,1,0:T(2,128)(2,1)S(1)}, u32[]{:S(2)}, u32[]{:S(2)}) %all-to-all-start.1) | async-done | bytes 524320 | tf_op jit(solution)/shard_map/all_to_all | solution.py:42
  133.5 0.5 reshape.130
  134.2 1.2 gather_fusion
  135.3 0.3 reshape.109
  135.7 1.4 multiply_reduce_fusion
  (21 shorter events, 1.2 us)
Async XLA Ops:
  6.5 51.7 %all-gather.2.cloned.1.call-start = ((), (), s32[]{:S(2)}) async-start(), calls=%async_computation.3 | async-start | bytes 2621440 | tf_op jit(solution)/shard_map/all_gather | solution.py:34
  36.5 69.7 %reduce-scatter.2.cloned.1.call-start = ((), (), s32[]{:S(2)}) async-start(), calls=%async_computation.4 | async-start | bytes 2621440 | tf_op jit(solution)/shard_map/reduce_scatter | solution.py:39
  58.2 6.6 %copy-start.1 = (bf16[1,512,2048]{2,1,0:T(8,128)(2,1)S(1)}, bf16[1,512,2048]{2,1,0:T(8,128)(2,1)}, u32[]{:S(2)}) copy-start(bf16[1,512,2048]{2,1,0:T(8,128)(2,1)} %all-gather.2.cloned.1.call-done) | copy-start | bytes 6291460
  108.0 11.2 %copy-start = (f32[128,2]{0,1:T(2,128)S(1)}, f32[128,2]{0,1:T(2,128)}, u32[]{:S(2)}) copy-start(f32[128,2]{0,1:T(2,128)} %param.10) | copy-start | bytes 3076
  113.7 19.8 %all-to-all-start.1 = ((bf16[8,2,16384]{2,1,0:T(2,128)(2,1)}), bf16[8,2,16384]{2,1,0:T(2,128)(2,1)S(1)}, u32[]{:S(2)}, u32[]{:S(2)}) async-start(bf16[8,2,16384]{2,1,0:T(2,128)(2,1)} %reshape.129), calls=%async_computation.2 | async-start | bytes 1048576 | tf_op jit(solution)/shard_map/all_to_all | solution.py:42
Sparse Core Ops, SparseCore 0:
  36.6 21.5 all-gather.1
  75.0 31.1 reduce-scatter.1
where the time goes:
time: 144 us
  waiting for transfers between devices  67.1 us (47%)
  blocking collectives  21.7 us (15%)
  matrix products  16.6 us (12%)
  between operations  13.5 us (9%)
  local copies, waits for them, and re-layouts  10.1 us (7%)
  other arithmetic  9.19 us (6%)
  starting transfers between devices  5.74 us (4%)
    reduce_scatter x1, waiting for transfers between devices, per_device(): lax.psum_scatter(partial_value.astype(jnp.bfloat16), 'tp', scatter_dimens...  31.3 us
    all_to_all x1, blocking collectives, per_device(): lax.all_to_all(outgoing, 'ep', split_axis=0, concat_axis=1, tiled=True)  21.7 us
    all_gather x1, waiting for transfers between devices, per_device(): piece = lax.all_gather(arrived, 'tp', axis=2, tiled=True)  21.5 us
    all_to_all x1, waiting for transfers between devices, per_device(): lax.all_to_all(summed, 'ep', split_axis=1, concat_axis=0, tiled=True)  14.2 us
    dot_general x1, matrix products, per_device(): jnp.einsum('erf,efd->erd', hidden, w_down, preferred_element_type=jnp.flo...  9.99 us
    dot_general x1, matrix products, per_device(): jnp.einsum('erd,edf->erf', piece, w_gate, preferred_element_type=jnp.floa...  6.59 us
    all_to_all x1, starting transfers between devices, per_device(): lax.all_to_all(summed, 'ep', split_axis=1, concat_axis=0, tiled=True)  5.51 us
    unnamed x1, other arithmetic  3.95 us
  transfers between devices with their start and end apart: 3, of which 3 were waited for; matrix products, arithmetic and copies ran while one was open for 0% of the time, Pallas kernels for 0%

commit v1 on v0

--- a/solution.py
+++ b/solution.py
@@ -31,7 +31,7 @@
     )
     outgoing = outgoing.reshape(experts, capacity, token_rows.shape[1])
     arrived = lax.all_to_all(outgoing, "ep", split_axis=0, concat_axis=1, tiled=True)
-    piece = lax.all_gather(arrived, "tp", axis=2, tiled=True)
+    piece = jnp.concatenate(lax.all_gather(arrived, "tp"), axis=2)
     gate_part = jnp.einsum("erd,edf->erf", piece, w_gate, preferred_element_type=jnp.float32)
     up_part = jnp.einsum("erd,edf->erf", piece, w_up, preferred_element_type=jnp.float32)
     hidden = (jax.nn.silu(gate_part) * up_part).astype(jnp.bfloat16)

time: 144 us -> 147 us (1.021)
  local copies, waits for them, and re-layouts: 10.1 us -> 12.8 us
    all_gather x0 -> x1, local copies, waits for them, and re-layouts: none -> 2.79 us  [per_device(): piece = jnp.concatenate(lax.all_gather(arrived, 'tp'), axis=2)]
    unnamed x10 -> x8, local copies, waits for them, and re-layouts: 3.23 us -> 3.23 us
where the time goes in v1:
time: 147 us; the launch traced here: 146 us
  waiting for transfers between devices  67.1 us (46%)
  blocking collectives  21.7 us (15%)
  matrix products  16.1 us (11%)
  between operations  13.5 us (9%)
  local copies, waits for them, and re-layouts  12.8 us (9%)
  other arithmetic  9.19 us (6%)
  starting transfers between devices  5.74 us (4%)
    reduce_scatter x1, waiting for transfers between devices, per_device(): lax.psum_scatter(partial_value.astype(jnp.bfloat16), 'tp', scatter_dimens...  31.3 us
    all_to_all x1, blocking collectives, per_device(): lax.all_to_all(outgoing, 'ep', split_axis=0, concat_axis=1, tiled=True)  21.7 us
    all_gather x1, waiting for transfers between devices, per_device(): piece = jnp.concatenate(lax.all_gather(arrived, 'tp'), axis=2)  21.5 us
    all_to_all x1, waiting for transfers between devices, per_device(): lax.all_to_all(summed, 'ep', split_axis=1, concat_axis=0, tiled=True)  14.2 us
    dot_general x1, matrix products, per_device(): jnp.einsum('erf,efd->erd', hidden, w_down, preferred_element_type=jnp.flo...  10.2 us
    dot_general x1, matrix products, per_device(): jnp.einsum('erd,edf->erf', piece, w_gate, preferred_element_type=jnp.floa...  5.88 us
    all_to_all x1, starting transfers between devices, per_device(): lax.all_to_all(summed, 'ep', split_axis=1, concat_axis=0, tiled=True)  5.51 us
    unnamed x1, other arithmetic  3.95 us
  transfers between devices with their start and end apart: 3, of which 3 were waited for; matrix products, arithmetic and copies ran while one was open for 0% of the time, Pallas kernels for 0%

profile of v1, /device:TPU:0, one launch (start us, length us, event | category | flops | bytes accessed | tf_op | source)
XLA Modules:
  0.0 146.1 jit_solution(932356380528511212)
XLA Ops:
  6.5 0.8 copy.26
  7.6 0.7 broadcast_multiply_fusion
  8.3 0.6 reduce-window.6
  9.4 1.2 fusion.14
  10.6 1.2 fusion.16
  11.9 0.6 broadcast_in_dim.5
  12.5 0.4 reshape.109
  13.0 1.7 %scatter_custom_fusion = bf16[512,512]{1,0:T(8,128)(2,1)S(1)} fusion(s32[256]{0:T(256)S(1)} %bitcast.50, bf16[256,2048]{1,0:T(8,128)(2,1)S(1)} %reshape.109, s32[]{:T(128)} %constant.12.clone.1, s32[]{:T(128)S(6)} %select_n.15, bf16[]{:T(256)} %constant.10.clone.1), kind=kCustom, calls=%fused_computation.18 | custom fusion | bytes 786442 | tf_op jit(solution)/shard_map/scatter | solution.py:30
  14.7 21.7 %all_to_all.8 = bf16[8,64,512]{2,1,0:T(8,128)(2,1)} all-to-all(bf16[8,64,512]{2,1,0:T(8,128)(2,1)S(1)} %bitcast.49), channel_id=1, replica_groups=mesh['ep'=8,'tp'=4] {'ep'}, dimensions={0} | all-to-all | bytes 1048576 | tf_op jit(solution)/shard_map/all_to_all | solution.py:33
  36.7 21.5 %all-gather.2.cloned.1.call-done = bf16[4,1,512,512]{3,2,1,0:T(8,128)(2,1)} async-done(((bf16[1,1,512,512]{3,2,1,0:T(8,128)(2,1)}), bf16[4,1,512,512]{3,2,1,0:T(8,128)(2,1)}) %all-gather.2.cloned.1.call-update) | async-done | bytes 2097168 | tf_op jit(solution)/shard_map/all_gather | solution.py:34
  58.2 2.8 %copy.28 = bf16[4,1,512,512]{2,3,0,1:T(8,128)(2,1)S(1)} copy(bf16[4,1,512,512]{3,2,1,0:T(8,128)(2,1)} %all-gather.2.cloned.1.call-done) | data formatting | bytes 4194304 | tf_op jit(solution)/shard_map/all_gather | solution.py:34
  61.0 5.9 %fusion.4 = f32[512,1024]{1,0:T(8,128)} fusion(bf16[512,2048]{0,1:T(8,128)(2,1)S(1)} %bitcast.46, bf16[1,2048,1024]{2,1,0:T(8,128)(2,1)} %param.11), kind=kOutput, calls=%fused_computation.6 | convolution fusion | flops 2147483648 | bytes 8388608 | tf_op jit(solution)/shard_map/erd,edf->erf/dot_general | solution.py:35
  66.9 10.2 %fusion.9 = bf16[1,512,2048]{2,1,0:T(8,128)(2,1)} fusion(bf16[1,1024,2048]{2,1,0:T(8,128)(2,1)} %param.13, f32[512,1024]{1,0:T(8,128)} %fusion.4, bf16[512,2048]{0,1:T(8,128)(2,1)S(1)} %bitcast.47, bf16[1,2048,1024]{2,1,0:T(8,128)(2,1)} %param.12), kind=kOutput, calls=%fused_computation.9 | convolution fusion | flops 4299161600 | bytes 14680064 | tf_op jit(solution)/shard_map/erf,efd->erd/dot_general | solution.py:38
  77.1 31.3 %reduce-scatter.2.cloned.1.call-done = bf16[1,512,512]{2,1,0:T(8,128)(2,1)} async-done(((bf16[1,512,2048]{2,1,0:T(8,128)(2,1)}), bf16[1,512,512]{2,1,0:T(8,128)(2,1)}) %reduce-scatter.2.cloned.1.call-update) | async-done | bytes 524304 | tf_op jit(solution)/shard_map/reduce_scatter | solution.py:39
  108.4 1.9 %copy.35 = bf16[1,512,512]{2,0,1:T(2,128)(2,1)S(1)} copy(bf16[1,512,512]{2,1,0:T(8,128)(2,1)} %reduce-scatter.2.cloned.1.call-done) | data formatting | bytes 1048576 | tf_op jit(solution)/shard_map/reduce_scatter | solution.py:39
  110.3 0.5 broadcast.73
  110.8 4.0 %reduce.2 = bf16[512,512]{1,0:T(8,128)(2,1)S(1)} reduce(bf16[512,1,512]{2,1,0:T(2,128)(2,1)S(1)} %bitcast.45, bf16[]{:T(256)} %broadcast.73), dimensions={1}, to_apply=%bitcast.42.reduce_sub_computation | reduce | bytes 1048578
  114.8 1.2 reshape.137
  115.9 5.5 %all-to-all-start.1 = ((bf16[8,2,16384]{2,1,0:T(2,128)(2,1)}), bf16[8,2,16384]{2,1,0:T(2,128)(2,1)S(1)}, u32[]{:S(2)}, u32[]{:S(2)}) async-start(bf16[8,2,16384]{2,1,0:T(2,128)(2,1)} %reshape.137), calls=%async_computation.2 | async-start | bytes 1048576 | tf_op jit(solution)/shard_map/all_to_all | solution.py:42
  121.6 14.2 %all-to-all-done.1 = bf16[8,2,16384]{2,1,0:T(2,128)(2,1)S(1)} async-done(((bf16[8,2,16384]{2,1,0:T(2,128)(2,1)}), bf16[8,2,16384]{2,1,0:T(2,128)(2,1)S(1)}, u32[]{:S(2)}, u32[]{:S(2)}) %all-to-all-start.1) | async-done | bytes 524320 | tf_op jit(solution)/shard_map/all_to_all | solution.py:42
  135.7 0.5 reshape.138
  136.4 1.2 gather_fusion
  137.6 0.3 reshape.117
  137.9 1.4 multiply_reduce_fusion
  (20 shorter events, 1.4 us)
Async XLA Ops:
  6.5 51.7 %all-gather.2.cloned.1.call-start = ((), (), s32[]{:S(2)}) async-start(), calls=%async_computation.3 | async-start | bytes 2621440 | tf_op jit(solution)/shard_map/all_gather | solution.py:34
  36.5 72.0 %reduce-scatter.2.cloned.1.call-start = ((), (), s32[]{:S(2)}) async-start(), calls=%async_computation.4 | async-start | bytes 2621440 | tf_op jit(solution)/shard_map/reduce_scatter | solution.py:39
  110.3 11.2 %copy-start = (f32[128,2]{0,1:T(2,128)S(1)}, f32[128,2]{0,1:T(2,128)}, u32[]{:S(2)}) copy-start(f32[128,2]{0,1:T(2,128)} %param.10) | copy-start | bytes 3076
  115.9 19.8 %all-to-all-start.1 = ((bf16[8,2,16384]{2,1,0:T(2,128)(2,1)}), bf16[8,2,16384]{2,1,0:T(2,128)(2,1)S(1)}, u32[]{:S(2)}, u32[]{:S(2)}) async-start(bf16[8,2,16384]{2,1,0:T(2,128)(2,1)} %reshape.137), calls=%async_computation.2 | async-start | bytes 1048576 | tf_op jit(solution)/shard_map/all_to_all | solution.py:42
Sparse Core Ops, SparseCore 0:
  36.6 21.5 all-gather.1
  77.2 31.1 reduce-scatter.1
